TPU v7x, 32 devices: a whole 2x2x4 slice. The times are simulated.
32 devices in a mesh: rep: 2 (over x), fs: 8 (over z, y), tp: 2 (over core).
Axes of the slice: x: 2, y: 2, z: 4, core: 2. Of those that a mesh axis runs over, the one named last changes fastest.
Arguments:
- tokens: bfloat16 [5120, 2048], P(('rep', 'fs')), may hold values from -6 to 6
- mixer_out: bfloat16 [5120, 2048], P(('rep', 'fs')), may hold values from -6 to 6
- gate_first: bfloat16 [2048, 2816], P('fs', 'tp'), may hold values from -0.125 to 0.125
- up_first: bfloat16 [2048, 2816], P('fs', 'tp'), may hold values from -0.125 to 0.125
- down_first: bfloat16 [2816, 2048], P('tp', 'fs'), may hold values from -0.3125 to 0.3125
- gate_second: bfloat16 [2048, 2816], P('fs', 'tp'), may hold values from -0.125 to 0.125
- up_second: bfloat16 [2048, 2816], P('fs', 'tp'), may hold values from -0.125 to 0.125
- down_second: bfloat16 [2816, 2048], P('tp', 'fs'), may hold values from -0.3125 to 0.3125
- gain_first: float32 [2048], replicated, may hold values from 0.1 to 1.9
- bias_first: float32 [2048], replicated, may hold values from -1.5 to 1.5
- gain_middle: float32 [2048], replicated, may hold values from 0.1 to 1.9
- bias_middle: float32 [2048], replicated, may hold values from -1.5 to 1.5
- gain_last: float32 [2048], replicated, may hold values from 0.1 to 1.9
- bias_last: float32 [2048], replicated, may hold values from -1.5 to 1.5
Outputs:
- layer_out: bfloat16 [5120, 2048], P(('rep', 'fs'))
All inputs are finite; a program needn't handle non-finite values.
Results may differ from a plain program's by a relative error of at most 0.014.
Values may be sent and summed in bfloat16 or wider, within the bound.
A program may use at most 64 MiB of HBM per device.

v0:
```python
import math
import jax
import jax.numpy as jnp
from jax import lax
from jax.sharding import PartitionSpec as P

residual_scale = math.sqrt(2.0)
norm_eps = 1e-05


def normalize(summed, scaling, offset):
    center = summed - jnp.mean(summed, axis=-1, keepdims=True)
    spread = jnp.mean(center * center, axis=-1, keepdims=True)
    return center * lax.rsqrt(spread + norm_eps) * scaling + offset


def add_columns(inputs, portion):
    return jnp.dot(inputs, portion, preferred_element_type=jnp.float32)


def project_in(inputs, gate_weight, up_weight):
    return (
        add_columns(inputs, lax.all_gather(gate_weight, "fs", axis=0, tiled=True)),
        add_columns(inputs, lax.all_gather(up_weight, "fs", axis=0, tiled=True)),
    )


def project_out(hidden, down_weight):
    return jnp.dot(
        hidden,
        lax.all_gather(down_weight, "fs", axis=1, tiled=True),
        preferred_element_type=jnp.float32,
    )


def half_step(inputs, gate_weight, up_weight, down_weight):
    gate, value = project_in(inputs, gate_weight, up_weight)
    hidden = (jax.nn.silu(gate) * value).astype(jnp.bfloat16)
    partials = project_out(hidden, down_weight)
    summed = lax.psum(partials.astype(jnp.bfloat16), "tp")
    return summed


def per_device(
    tokens,
    mixer_out,
    gate_first,
    up_first,
    down_first,
    gate_second,
    up_second,
    down_second,
    gain_first,
    bias_first,
    gain_middle,
    bias_middle,
    gain_last,
    bias_last,
):
    first_branch = half_step(tokens, gate_first, up_first, down_first)
    first_norm = normalize(
        residual_scale * tokens.astype(jnp.float32) + 0.5 * first_branch.astype(jnp.float32),
        gain_first,
        bias_first,
    ).astype(jnp.bfloat16)
    middle_norm = normalize(
        residual_scale * first_norm.astype(jnp.float32) + mixer_out.astype(jnp.float32),
        gain_middle,
        bias_middle,
    ).astype(jnp.bfloat16)
    second_branch = half_step(middle_norm, gate_second, up_second, down_second)
    finished = normalize(
        residual_scale * middle_norm.astype(jnp.float32) + 0.5 * second_branch.astype(jnp.float32),
        gain_last,
        bias_last,
    ).astype(jnp.bfloat16)
    return finished


def solution(mesh):
    return jax.shard_map(
        per_device,
        mesh=mesh,
        in_specs=(
            P(("rep", "fs"), None),
            P(("rep", "fs"), None),
            P("fs", "tp"),
            P("fs", "tp"),
            P("tp", "fs"),
            P("fs", "tp"),
            P("fs", "tp"),
            P("tp", "fs"),
            P(),
            P(),
            P(),
            P(),
            P(),
            P(),
        ),
        out_specs=P(("rep", "fs"), None),
        check_vma=False,
    )
```

profile of v0, /device:TPU:0, one launch (start us, length us, event | category | flops | bytes accessed | tf_op | source)
XLA Modules:
  0.0 639.6 jit_solution(13720102844049315975)
XLA Ops:
  6.5 0.7 all-gather.7.cloned.1.call-update
  7.3 0.7 all-gather.11.cloned.1.call-update
  8.0 0.0 all-gather.9.cloned.1.call-start
  8.1 0.7 all-gather.9.cloned.1.call-update
  8.8 0.0 all-reduce.3.cloned.1.call-start
  8.8 95.8 %all-gather.7.cloned.1.call-done = bf16[2048,1408]{1,0:T(8,128)(2,1)} async-done(((bf16[256,1408]{1,0:T(8,128)(2,1)}), bf16[2048,1408]{1,0:T(8,128)(2,1)}) %all-gather.7.cloned.1.call-update) | async-done | bytes 5767184 | tf_op jit(solution)/shard_map/all_gather | solution.py:23
  104.6 5.2 fusion.7
  109.8 88.2 %all-gather.11.cloned.1.call-done = bf16[1408,2048]{1,0:T(8,128)(2,1)} async-done(((bf16[1408,256]{1,0:T(8,128)(2,1)}), bf16[1408,2048]{1,0:T(8,128)(2,1)}) %all-gather.11.cloned.1.call-update) | async-done | bytes 5767184 | tf_op jit(solution)/shard_map/all_gather | solution.py:31
  198.0 92.7 %all-gather.9.cloned.1.call-done = bf16[2048,1408]{1,0:T(8,128)(2,1)} async-done(((bf16[256,1408]{1,0:T(8,128)(2,1)}), bf16[2048,1408]{1,0:T(8,128)(2,1)}) %all-gather.9.cloned.1.call-update) | async-done | bytes 5767184 | tf_op jit(solution)/shard_map/all_gather | solution.py:24
  290.7 9.7 %convolution_convert_fusion.1 = bf16[320,2048]{1,0:T(8,128)(2,1)} fusion(bf16[1408,2048]{1,0:T(8,128)(2,1)} %all-gather.11.cloned.1.call-done, bf16[320,2048]{1,0:T(8,128)(2,1)S(1)} %copy-done.2, bf16[2048,1408]{1,0:T(8,128)(2,1)} %all-gather.9.cloned.1.call-done, f32[320,1408]{1,0:T(8,128)S(1)} %fusion.7), kind=kOutput, calls=%fused_computation.3 | convolution fusion | flops 3694346240 | bytes 15958016 | tf_op jit(solution)/shard_map/dot_general | solution.py:29
  300.4 0.0 all-gather.13.cloned.1.call-start
  300.4 0.5 all-gather.13.cloned.1.call-update
  301.0 0.0 all-gather.15.cloned.1.call-start
  301.0 0.5 all-gather.15.cloned.1.call-update
  301.5 0.0 all-gather.17.cloned.1.call-start
  301.6 0.7 all-gather.17.cloned.1.call-update
  302.3 0.2 all-reduce.5.cloned.1.call-start
  302.5 16.1 %all-reduce.3.cloned.1.call-done = bf16[320,2048]{1,0:T(8,128)(2,1)} async-done(((bf16[320,2048]{1,0:T(8,128)(2,1)}), bf16[320,2048]{1,0:T(8,128)(2,1)}) %all-reduce.3.cloned.1.call-update) | async-done | bytes 1310736 | tf_op jit(solution)/shard_map/psum | solution.py:40
  318.6 2.0 fusion.3
  320.6 0.8 multiply_reduce_fusion.2
  321.5 1.3 fusion.2
  322.8 0.7 multiply_reduce_fusion.1
  323.5 0.8 add_convert_fusion.1
  324.3 89.9 %all-gather.13.cloned.1.call-done = bf16[2048,1408]{1,0:T(8,128)(2,1)} async-done(((bf16[256,1408]{1,0:T(8,128)(2,1)}), bf16[2048,1408]{1,0:T(8,128)(2,1)}) %all-gather.13.cloned.1.call-update) | async-done | bytes 5767184 | tf_op jit(solution)/shard_map/all_gather | solution.py:23
  414.2 4.8 fusion.8
  419.0 87.7 %all-gather.15.cloned.1.call-done = bf16[2048,1408]{1,0:T(8,128)(2,1)} async-done(((bf16[256,1408]{1,0:T(8,128)(2,1)}), bf16[2048,1408]{1,0:T(8,128)(2,1)}) %all-gather.15.cloned.1.call-update) | async-done | bytes 5767184 | tf_op jit(solution)/shard_map/all_gather | solution.py:24
  506.7 93.4 %all-gather.17.cloned.1.call-done = bf16[1408,2048]{1,0:T(8,128)(2,1)} async-done(((bf16[1408,256]{1,0:T(8,128)(2,1)}), bf16[1408,2048]{1,0:T(8,128)(2,1)}) %all-gather.17.cloned.1.call-update) | async-done | bytes 5767184 | tf_op jit(solution)/shard_map/all_gather | solution.py:31
  600.1 9.7 %convolution_convert_fusion = bf16[320,2048]{1,0:T(8,128)(2,1)} fusion(bf16[1408,2048]{1,0:T(8,128)(2,1)} %all-gather.17.cloned.1.call-done, bf16[320,2048]{1,0:T(8,128)(2,1)S(1)} %add_convert_fusion.1, bf16[2048,1408]{1,0:T(8,128)(2,1)} %all-gather.15.cloned.1.call-done, f32[320,1408]{1,0:T(8,128)S(1)} %fusion.8), kind=kOutput, calls=%fused_computation.2 | convolution fusion | flops 3694346240 | bytes 15958016 | tf_op jit(solution)/shard_map/dot_general | solution.py:29
  609.8 18.2 %all-reduce.5.cloned.1.call-done = bf16[320,2048]{1,0:T(8,128)(2,1)} async-done(((bf16[320,2048]{1,0:T(8,128)(2,1)}), bf16[320,2048]{1,0:T(8,128)(2,1)}) %all-reduce.5.cloned.1.call-update) | async-done | bytes 1310736 | tf_op jit(solution)/shard_map/psum | solution.py:40
  628.0 2.0 fusion.4
  630.0 0.8 multiply_reduce_fusion
  630.9 1.9 add_convert_fusion
  (30 shorter events, 0.2 us)
Async XLA Ops:
  6.5 98.0 %all-gather.7.cloned.1.call-start = ((), (), s32[]{:S(2)}) async-start(), calls=%async_computation | async-start | bytes 6488064 | tf_op jit(solution)/shard_map/all_gather | solution.py:23
  7.3 190.7 %all-gather.11.cloned.1.call-start = ((), (), s32[]{:S(2)}) async-start(), calls=%async_computation.2 | async-start | bytes 6488064 | tf_op jit(solution)/shard_map/all_gather | solution.py:31
  8.0 282.7 %all-gather.9.cloned.1.call-start = ((), (), s32[]{:S(2)}) async-start(), calls=%async_computation.1 | async-start | bytes 6488064 | tf_op jit(solution)/shard_map/all_gather | solution.py:24
  8.7 281.9 %copy-start.2 = (bf16[320,2048]{1,0:T(8,128)(2,1)S(1)}, bf16[320,2048]{1,0:T(8,128)(2,1)}, u32[]{:S(2)}) copy-start(bf16[320,2048]{1,0:T(8,128)(2,1)} %param.14) | copy-start | bytes 3932164
  8.8 309.8 %all-reduce.3.cloned.1.call-start = ((), (), s32[]{:S(2)}) async-start(), calls=%async_computation.3 | async-start | bytes 2621440 | tf_op jit(solution)/shard_map/psum | solution.py:40
  300.4 113.8 %all-gather.13.cloned.1.call-start = ((), (), s32[]{:S(2)}) async-start(), calls=%async_computation.4 | async-start | bytes 6488064 | tf_op jit(solution)/shard_map/all_gather | solution.py:23
  301.0 205.8 %all-gather.15.cloned.1.call-start = ((), (), s32[]{:S(2)}) async-start(), calls=%async_computation.5 | async-start | bytes 6488064 | tf_op jit(solution)/shard_map/all_gather | solution.py:24
  301.5 298.6 %all-gather.17.cloned.1.call-start = ((), (), s32[]{:S(2)}) async-start(), calls=%async_computation.6 | async-start | bytes 6488064 | tf_op jit(solution)/shard_map/all_gather | solution.py:31
  301.6 19.9 %copy-start.4 = (f32[2048]{0:T(1024)S(1)}, f32[2048]{0:T(1024)}, u32[]{:S(2)}) copy-start(f32[2048]{0:T(1024)} %param.23) | copy-start | bytes 24580
  301.6 19.9 %copy-start.5 = (f32[2048]{0:T(1024)S(1)}, f32[2048]{0:T(1024)}, u32[]{:S(2)}) copy-start(f32[2048]{0:T(1024)} %param.22) | copy-start | bytes 24580
  302.3 19.2 %copy-start.1 = (bf16[320,2048]{1,0:T(8,128)(2,1)S(1)}, bf16[320,2048]{1,0:T(8,128)(2,1)}, u32[]{:S(2)}) copy-start(bf16[320,2048]{1,0:T(8,128)(2,1)} %param.15) | copy-start | bytes 3932164
  302.3 325.7 %all-reduce.5.cloned.1.call-start = ((), (), s32[]{:S(2)}) async-start(), calls=%async_computation.7 | async-start | bytes 2621440 | tf_op jit(solution)/shard_map/psum | solution.py:40
  318.6 2.0 copy-start.3
  322.8 0.7 copy-start.6
  322.8 0.7 copy-start.7
  609.8 21.0 %copy-start.8 = (f32[2048]{0:T(1024)S(1)}, f32[2048]{0:T(1024)}, u32[]{:S(2)}) copy-start(f32[2048]{0:T(1024)} %param.27) | copy-start | bytes 24580
  609.8 21.0 %copy-start.9 = (f32[2048]{0:T(1024)S(1)}, f32[2048]{0:T(1024)}, u32[]{:S(2)}) copy-start(f32[2048]{0:T(1024)} %param.26) | copy-start | bytes 24580
  628.0 2.0 copy-start
Sparse Core Ops, SparseCore 0:
  9.5 95.0 all-gather.6
  106.6 91.3 all-gather.10
  200.2 90.4 all-gather.8
  300.5 18.0 all-reduce.2
  320.6 93.4 all-gather.12
  416.2 90.4 all-gather.14
  508.8 91.2 all-gather.16
  609.9 18.0 all-reduce.4
where the time goes:
time: 640 us
  waiting for transfers between devices  586 us (92%)
  matrix products  29.4 us (5%)
  between operations  13.6 us (2%)
  other arithmetic  10.4 us (2%)
    all_gather x2, waiting for transfers between devices, project_in(): lax.all_gather(gate_weight, 'fs', axis=0, tiled=True)  186 us
    all_gather x2, waiting for transfers between devices, project_out(): lax.all_gather(down_weight, 'fs', axis=1, tiled=True)  182 us
    all_gather x2, waiting for transfers between devices, project_in(): lax.all_gather(up_weight, 'fs', axis=0, tiled=True)  180 us
    psum x2, waiting for transfers between devices, half_step(): summed = lax.psum(partials.astype(jnp.bfloat16), 'tp')  34.3 us
    dot_general x2, matrix products, project_out(): jnp.dot(hidden, lax.all_gather(down_weight, 'fs', axis=1, tiled=True), pr...  19.3 us
  transfers between devices with their start and end apart: 8, of which 8 were waited for; matrix products, arithmetic and copies ran while one was open for 2% of the time, Pallas kernels for 0%

commit v1 on v0

--- a/solution.py
+++ b/solution.py
@@ -6,6 +6,17 @@
 
 residual_scale = math.sqrt(2.0)
 norm_eps = 1e-05
+
+
+def gather_around(x, axis, dim):
+    ways = lax.axis_size(axis)
+    pieces = [x]
+    for far in range(1, ways):
+        pieces.append(
+            lax.ppermute(pieces[far - 1], axis, [(d, (d - 1) % ways) for d in range(ways)])
+        )
+    line = jnp.concatenate(pieces, axis=dim)
+    return jnp.roll(line, lax.axis_index(axis) * x.shape[dim], axis=dim)
 
 
 def normalize(summed, scaling, offset):
@@ -20,7 +31,7 @@
 
 def project_in(inputs, gate_weight, up_weight):
     return (
-        add_columns(inputs, lax.all_gather(gate_weight, "fs", axis=0, tiled=True)),
+        add_columns(inputs, gather_around(gate_weight, "fs", 0)),
         add_columns(inputs, lax.all_gather(up_weight, "fs", axis=0, tiled=True)),
     )
 

time: 640 us -> 607 us (0.948)
  waiting for transfers between devices: 586 us -> 465 us
  starting transfers between devices: 0.45 us -> 69.1 us
  local copies, waits for them, and re-layouts: 0.05 us -> 17.1 us
    ppermute x0 -> x14, waiting for transfers between devices: none -> 330 us  [gather_around(): lax.ppermute(pieces[far - 1], axis, [(d, (d - 1) % ways) for d in range(w...]
    all_gather x2 -> x0, waiting for transfers between devices: 186 us -> none  [project_in(): lax.all_gather(gate_weight, 'fs', axis=0, tiled=True)]
    all_gather x2, waiting for transfers between devices: 180 us -> 0.02 us  [project_in(): lax.all_gather(up_weight, 'fs', axis=0, tiled=True)]
    ppermute x0 -> x14, starting transfers between devices: none -> 68.9 us  [gather_around(): lax.ppermute(pieces[far - 1], axis, [(d, (d - 1) % ways) for d in range(w...]
    all_gather x2, waiting for transfers between devices: 182 us -> 115 us  [project_out(): lax.all_gather(down_weight, 'fs', axis=1, tiled=True)]
    psum x2, waiting for transfers between devices: 34.3 us -> 18.3 us  [half_step(): summed = lax.psum(partials.astype(jnp.bfloat16), 'tp')]
    unnamed x20 -> x36, local copies, waits for them, and re-layouts: 0.05 us -> 15.3 us
  transfers between devices with their start and end apart: 8 -> 20, of which waited for: 8 -> 17; matrix products, arithmetic and copies ran while one was open for 2% -> 5% of each run, Pallas kernels for 0% -> 0%
where the time goes in v1:
time: 607 us
  waiting for transfers between devices  465 us (77%)
  starting transfers between devices  69.1 us (11%)
  matrix products  31 us (5%)
  local copies, waits for them, and re-layouts  17.1 us (3%)
  between operations  13.6 us (2%)
  other arithmetic  10.4 us (2%)
    ppermute x14, waiting for transfers between devices, gather_around(): lax.ppermute(pieces[far - 1], axis, [(d, (d - 1) % ways) for d in range(w...  330 us
    all_gather x2, waiting for transfers between devices, project_out(): lax.all_gather(down_weight, 'fs', axis=1, tiled=True)  115 us
    ppermute x14, starting transfers between devices, gather_around(): lax.ppermute(pieces[far - 1], axis, [(d, (d - 1) % ways) for d in range(w...  68.9 us
    dot_general x2, matrix products, project_out(): jnp.dot(hidden, lax.all_gather(down_weight, 'fs', axis=1, tiled=True), pr...  21.4 us
    psum x2, waiting for transfers between devices, half_step(): summed = lax.psum(partials.astype(jnp.bfloat16), 'tp')  18.3 us
    unnamed x36, local copies, waits for them, and re-layouts  15.3 us
  transfers between devices with their start and end apart: 20, of which 17 were waited for; matrix products, arithmetic and copies ran while one was open for 5% of the time, Pallas kernels for 0%

profile of v1, /device:TPU:0, one launch (start us, length us, event | category | flops | bytes accessed | tf_op | source)
XLA Modules:
  0.0 606.6 jit_solution(6820558270943710014)
XLA Ops:
  8.1 6.1 %collective-permute-start = (bf16[256,1408]{1,0:T(8,128)(2,1)}, bf16[256,1408]{1,0:T(8,128)(2,1)S(1)}, u32[]{:S(2)}, u32[]{:S(2)}) collective-permute-start(bf16[256,1408]{1,0:T(8,128)(2,1)} %param.18), channel_id=1, source_target_pairs={{0,14},{2,0},{4,2},{6,4},{8,6},{10,8},{12,10},{14,12},{1,15},{3,1}... | collective-permute-start | bytes 2162696 | tf_op jit(solution)/shard_map/ppermute | solution.py:16
  14.1 25.2 %collective-permute-done = bf16[256,1408]{1,0:T(8,128)(2,1)S(1)} collective-permute-done((bf16[256,1408]{1,0:T(8,128)(2,1)}, bf16[256,1408]{1,0:T(8,128)(2,1)S(1)}, u32[]{:S(2)}, u32[]{:S(2)}) %collective-permute-start) | collective-permute-done | bytes 720928 | tf_op jit(solution)/shard_map/ppermute | solution.py:16
  39.4 5.1 collective-permute-start.1
  44.4 24.0 %collective-permute-done.1 = bf16[256,1408]{1,0:T(8,128)(2,1)S(1)} collective-permute-done((bf16[256,1408]{1,0:T(8,128)(2,1)S(1)}, bf16[256,1408]{1,0:T(8,128)(2,1)S(1)}, u32[]{:S(2)}, u32[]{:S(2)}) %collective-permute-start.1) | collective-permute-done | bytes 720928 | tf_op jit(solution)/shard_map/ppermute | solution.py:16
  68.4 5.2 collective-permute-start.2
  73.6 29.9 %collective-permute-done.2 = bf16[256,1408]{1,0:T(8,128)(2,1)S(1)} collective-permute-done((bf16[256,1408]{1,0:T(8,128)(2,1)S(1)}, bf16[256,1408]{1,0:T(8,128)(2,1)S(1)}, u32[]{:S(2)}, u32[]{:S(2)}) %collective-permute-start.2) | collective-permute-done | bytes 720928 | tf_op jit(solution)/shard_map/ppermute | solution.py:16
  103.5 5.2 collective-permute-start.3
  108.7 30.2 %collective-permute-done.3 = bf16[256,1408]{1,0:T(8,128)(2,1)S(1)} collective-permute-done((bf16[256,1408]{1,0:T(8,128)(2,1)S(1)}, bf16[256,1408]{1,0:T(8,128)(2,1)S(1)}, u32[]{:S(2)}, u32[]{:S(2)}) %collective-permute-start.3) | collective-permute-done | bytes 720928 | tf_op jit(solution)/shard_map/ppermute | solution.py:16
  138.9 5.2 collective-permute-start.4
  146.1 19.1 %collective-permute-done.4 = bf16[256,1408]{1,0:T(8,128)(2,1)} collective-permute-done((bf16[256,1408]{1,0:T(8,128)(2,1)S(1)}, bf16[256,1408]{1,0:T(8,128)(2,1)}, u32[]{:S(2)}, u32[]{:S(2)}) %collective-permute-start.4) | collective-permute-done | bytes 720928 | tf_op jit(solution)/shard_map/ppermute | solution.py:16
  165.2 5.3 collective-permute-start.5
  173.3 22.4 %collective-permute-done.5 = bf16[256,1408]{1,0:T(8,128)(2,1)S(1)} collective-permute-done((bf16[256,1408]{1,0:T(8,128)(2,1)}, bf16[256,1408]{1,0:T(8,128)(2,1)S(1)}, u32[]{:S(2)}, u32[]{:S(2)}) %collective-permute-start.5) | collective-permute-done | bytes 720928 | tf_op jit(solution)/shard_map/ppermute | solution.py:16
  195.7 5.1 collective-permute-start.6
  204.7 18.1 %collective-permute-done.6 = bf16[256,1408]{1,0:T(8,128)(2,1)S(1)} collective-permute-done((bf16[256,1408]{1,0:T(8,128)(2,1)S(1)}, bf16[256,1408]{1,0:T(8,128)(2,1)S(1)}, u32[]{:S(2)}, u32[]{:S(2)}) %collective-permute-start.6) | collective-permute-done | bytes 720928 | tf_op jit(solution)/shard_map/ppermute | solution.py:16
  228.5 53.3 %all-gather.7.cloned.1.call-done = bf16[1408,2048]{1,0:T(8,128)(2,1)} async-done(((bf16[1408,256]{1,0:T(8,128)(2,1)}), bf16[1408,2048]{1,0:T(8,128)(2,1)}) %all-gather.7.cloned.1.call-update) | async-done | bytes 5767184 | tf_op jit(solution)/shard_map/all_gather | solution.py:42
  281.8 10.7 %convolution_convert_fusion.1 = bf16[320,2048]{1,0:T(8,128)(2,1)} fusion(bf16[1408,2048]{1,0:T(8,128)(2,1)} %all-gather.7.cloned.1.call-done, f32[320,1408]{1,0:T(8,128)S(1)} %fusion.32, bf16[320,2048]{1,0:T(8,128)(2,1)S(1)} %copy-done.2, s32[]{:T(128)S(6)} %select_n.13, bf16[2048,1408]{1,0:T(8,128)(2,1)} %constant_dynamic-update-slice_fusion), kind=kOutput, calls=%fused_computation.10 | convolution fusion | flops 3705880576 | bytes 15958020 | tf_op jit(solution)/shard_map/dot_general | solution.py:40
  295.3 16.2 %collective-permute-done.7 = bf16[256,1408]{1,0:T(8,128)(2,1)S(1)} collective-permute-done((bf16[256,1408]{1,0:T(8,128)(2,1)S(1)}, bf16[256,1408]{1,0:T(8,128)(2,1)S(1)}, u32[]{:S(2)}, u32[]{:S(2)}) %collective-permute-start.7) | collective-permute-done | bytes 720928 | tf_op jit(solution)/shard_map/ppermute | solution.py:16
  316.0 24.0 %collective-permute-done.8 = bf16[256,1408]{1,0:T(8,128)(2,1)S(1)} collective-permute-done((bf16[256,1408]{1,0:T(8,128)(2,1)S(1)}, bf16[256,1408]{1,0:T(8,128)(2,1)S(1)}, u32[]{:S(2)}, u32[]{:S(2)}) %collective-permute-start.8) | collective-permute-done | bytes 720928 | tf_op jit(solution)/shard_map/ppermute | solution.py:16
  340.0 5.2 collective-permute-start.9
  345.2 24.1 %collective-permute-done.9 = bf16[256,1408]{1,0:T(8,128)(2,1)S(1)} collective-permute-done((bf16[256,1408]{1,0:T(8,128)(2,1)S(1)}, bf16[256,1408]{1,0:T(8,128)(2,1)S(1)}, u32[]{:S(2)}, u32[]{:S(2)}) %collective-permute-start.9) | collective-permute-done | bytes 720928 | tf_op jit(solution)/shard_map/ppermute | solution.py:16
  369.2 5.2 collective-permute-start.10
  374.4 29.9 %collective-permute-done.10 = bf16[256,1408]{1,0:T(8,128)(2,1)S(1)} collective-permute-done((bf16[256,1408]{1,0:T(8,128)(2,1)S(1)}, bf16[256,1408]{1,0:T(8,128)(2,1)S(1)}, u32[]{:S(2)}, u32[]{:S(2)}) %collective-permute-start.10) | collective-permute-done | bytes 720928 | tf_op jit(solution)/shard_map/ppermute | solution.py:16
  404.3 5.2 collective-permute-start.11
  410.4 29.2 %collective-permute-done.11 = bf16[256,1408]{1,0:T(8,128)(2,1)S(1)} collective-permute-done((bf16[256,1408]{1,0:T(8,128)(2,1)S(1)}, bf16[256,1408]{1,0:T(8,128)(2,1)S(1)}, u32[]{:S(2)}, u32[]{:S(2)}) %collective-permute-start.11) | collective-permute-done | bytes 720928 | tf_op jit(solution)/shard_map/ppermute | solution.py:16
  439.7 5.2 collective-permute-start.12
  447.6 17.6 %collective-permute-done.12 = bf16[256,1408]{1,0:T(8,128)(2,1)S(1)} collective-permute-done((bf16[256,1408]{1,0:T(8,128)(2,1)S(1)}, bf16[256,1408]{1,0:T(8,128)(2,1)S(1)}, u32[]{:S(2)}, u32[]{:S(2)}) %collective-permute-start.12) | collective-permute-done | bytes 720928 | tf_op jit(solution)/shard_map/ppermute | solution.py:16
  465.2 5.2 collective-permute-start.13
  473.2 19.9 %collective-permute-done.13 = bf16[256,1408]{1,0:T(8,128)(2,1)S(1)} collective-permute-done((bf16[256,1408]{1,0:T(8,128)(2,1)S(1)}, bf16[256,1408]{1,0:T(8,128)(2,1)S(1)}, u32[]{:S(2)}, u32[]{:S(2)}) %collective-permute-start.13) | collective-permute-done | bytes 720928 | tf_op jit(solution)/shard_map/ppermute | solution.py:16
  499.8 4.8 fusion.33
  504.6 61.3 %all-gather.11.cloned.1.call-done = bf16[1408,2048]{1,0:T(8,128)(2,1)} async-done(((bf16[1408,256]{1,0:T(8,128)(2,1)}), bf16[1408,2048]{1,0:T(8,128)(2,1)}) %all-gather.11.cloned.1.call-update) | async-done | bytes 5767184 | tf_op jit(solution)/shard_map/all_gather | solution.py:42
  566.0 10.7 %convolution_convert_fusion = bf16[320,2048]{1,0:T(8,128)(2,1)} fusion(bf16[1408,2048]{1,0:T(8,128)(2,1)} %all-gather.11.cloned.1.call-done, f32[320,1408]{1,0:T(8,128)S(1)} %fusion.33, bf16[320,2048]{1,0:T(8,128)(2,1)S(1)} %add_convert_fusion.1, s32[]{:T(128)S(6)} %select_n.13, bf16[2048,1408]{1,0:T(8,128)(2,1)} %constant_dynamic-update-slice_fusion.8), kind=kOutput, calls=%fused_computation.9 | convolution fusion | flops 3705880576 | bytes 15958020 | tf_op jit(solution)/shard_map/dot_general | solution.py:40
  576.7 18.3 %all-reduce.5.cloned.1.call-done = bf16[320,2048]{1,0:T(8,128)(2,1)} async-done(((bf16[320,2048]{1,0:T(8,128)(2,1)}), bf16[320,2048]{1,0:T(8,128)(2,1)}) %all-reduce.5.cloned.1.call-update) | async-done | bytes 1310736 | tf_op jit(solution)/shard_map/psum | solution.py:51
  (70 shorter events, 41.0 us)
Async XLA Ops:
  6.5 217.1 %all-gather.5.cloned.1.call-start = ((), (), s32[]{:S(2)}) async-start(), calls=%async_computation | async-start | bytes 6488064 | tf_op jit(solution)/shard_map/all_gather | solution.py:35
  7.3 274.6 %all-gather.7.cloned.1.call-start = ((), (), s32[]{:S(2)}) async-start(), calls=%async_computation.1 | async-start | bytes 6488064 | tf_op jit(solution)/shard_map/all_gather | solution.py:42
  8.0 486.0 %all-reduce.3.cloned.1.call-start = ((), (), s32[]{:S(2)}) async-start(), calls=%async_computation.2 | async-start | bytes 2621440 | tf_op jit(solution)/shard_map/psum | solution.py:51
  8.1 31.3 %collective-permute-start = (bf16[256,1408]{1,0:T(8,128)(2,1)}, bf16[256,1408]{1,0:T(8,128)(2,1)S(1)}, u32[]{:S(2)}, u32[]{:S(2)}) collective-permute-start(bf16[256,1408]{1,0:T(8,128)(2,1)} %param.18), channel_id=1, source_target_pairs={{0,14},{2,0},{4,2},{6,4},{8,6},{10,8},{12,10},{14,12},{1,15},{3,1}... | collective-permute-start | bytes 2162696 | tf_op jit(solution)/shard_map/ppermute | solution.py:16
  39.4 29.0 %collective-permute-start.1 = (bf16[256,1408]{1,0:T(8,128)(2,1)S(1)}, bf16[256,1408]{1,0:T(8,128)(2,1)S(1)}, u32[]{:S(2)}, u32[]{:S(2)}) collective-permute-start(bf16[256,1408]{1,0:T(8,128)(2,1)S(1)} %collective-permute-done), channel_id=1, source_target_pairs={{0,14},{2,0},{4,2},{6,4},{8,6},{10,8},{12,10},{14,12},{1,15},{3,1}... | collective-permute-start | bytes 2162696 | tf_op jit(solution)/shard_map/ppermute | solution.py:16
  68.4 35.1 %collective-permute-start.2 = (bf16[256,1408]{1,0:T(8,128)(2,1)S(1)}, bf16[256,1408]{1,0:T(8,128)(2,1)S(1)}, u32[]{:S(2)}, u32[]{:S(2)}) collective-permute-start(bf16[256,1408]{1,0:T(8,128)(2,1)S(1)} %collective-permute-done.1), channel_id=1, source_target_pairs={{0,14},{2,0},{4,2},{6,4},{8,6},{10,8},{12,10},{14,12},{1,15},{3,1}... | collective-permute-start | bytes 2162696 | tf_op jit(solution)/shard_map/ppermute | solution.py:16
  103.5 35.4 %collective-permute-start.3 = (bf16[256,1408]{1,0:T(8,128)(2,1)S(1)}, bf16[256,1408]{1,0:T(8,128)(2,1)S(1)}, u32[]{:S(2)}, u32[]{:S(2)}) collective-permute-start(bf16[256,1408]{1,0:T(8,128)(2,1)S(1)} %collective-permute-done.2), channel_id=1, source_target_pairs={{0,14},{2,0},{4,2},{6,4},{8,6},{10,8},{12,10},{14,12},{1,15},{3,1}... | collective-permute-start | bytes 2162696 | tf_op jit(solution)/shard_map/ppermute | solution.py:16
  138.9 26.3 %collective-permute-start.4 = (bf16[256,1408]{1,0:T(8,128)(2,1)S(1)}, bf16[256,1408]{1,0:T(8,128)(2,1)}, u32[]{:S(2)}, u32[]{:S(2)}) collective-permute-start(bf16[256,1408]{1,0:T(8,128)(2,1)S(1)} %collective-permute-done.3), channel_id=1, source_target_pairs={{0,14},{2,0},{4,2},{6,4},{8,6},{10,8},{12,10},{14,12},{1,15},{3,1}... | collective-permute-start | bytes 2162696 | tf_op jit(solution)/shard_map/ppermute | solution.py:16
  165.2 30.5 %collective-permute-start.5 = (bf16[256,1408]{1,0:T(8,128)(2,1)}, bf16[256,1408]{1,0:T(8,128)(2,1)S(1)}, u32[]{:S(2)}, u32[]{:S(2)}) collective-permute-start(bf16[256,1408]{1,0:T(8,128)(2,1)} %collective-permute-done.4), channel_id=1, source_target_pairs={{0,14},{2,0},{4,2},{6,4},{8,6},{10,8},{12,10},{14,12},{1,15},{3,1}... | collective-permute-start | bytes 2162696 | tf_op jit(solution)/shard_map/ppermute | solution.py:16
  173.3 50.4 %copy-start.2 = (bf16[320,2048]{1,0:T(8,128)(2,1)S(1)}, bf16[320,2048]{1,0:T(8,128)(2,1)}, u32[]{:S(2)}) copy-start(bf16[320,2048]{1,0:T(8,128)(2,1)} %param.16) | copy-start | bytes 3932164
  195.7 27.0 %collective-permute-start.6 = (bf16[256,1408]{1,0:T(8,128)(2,1)S(1)}, bf16[256,1408]{1,0:T(8,128)(2,1)S(1)}, u32[]{:S(2)}, u32[]{:S(2)}) collective-permute-start(bf16[256,1408]{1,0:T(8,128)(2,1)S(1)} %collective-permute-done.5), channel_id=1, source_target_pairs={{0,14},{2,0},{4,2},{6,4},{8,6},{10,8},{12,10},{14,12},{1,15},{3,1}... | collective-permute-start | bytes 2162696 | tf_op jit(solution)/shard_map/ppermute | solution.py:16
  292.5 1.2 copy-start.4
  292.5 207.3 %all-gather.9.cloned.1.call-start = ((), (), s32[]{:S(2)}) async-start(), calls=%async_computation.3 | async-start | bytes 6488064 | tf_op jit(solution)/shard_map/all_gather | solution.py:35
  293.1 272.9 %all-gather.11.cloned.1.call-start = ((), (), s32[]{:S(2)}) async-start(), calls=%async_computation.4 | async-start | bytes 6488064 | tf_op jit(solution)/shard_map/all_gather | solution.py:42
  293.7 301.3 %all-reduce.5.cloned.1.call-start = ((), (), s32[]{:S(2)}) async-start(), calls=%async_computation.5 | async-start | bytes 2621440 | tf_op jit(solution)/shard_map/psum | solution.py:51
  293.7 17.8 %collective-permute-start.7 = (bf16[256,1408]{1,0:T(8,128)(2,1)S(1)}, bf16[256,1408]{1,0:T(8,128)(2,1)S(1)}, u32[]{:S(2)}, u32[]{:S(2)}) collective-permute-start(bf16[256,1408]{1,0:T(8,128)(2,1)S(1)} %copy-done.4), channel_id=1, source_target_pairs={{0,14},{2,0},{4,2},{6,4},{8,6},{10,8},{12,10},{14,12},{1,15},{3,1}... | collective-permute-start | bytes 2162696 | tf_op jit(solution)/shard_map/ppermute | solution.py:16
  311.5 28.5 %collective-permute-start.8 = (bf16[256,1408]{1,0:T(8,128)(2,1)S(1)}, bf16[256,1408]{1,0:T(8,128)(2,1)S(1)}, u32[]{:S(2)}, u32[]{:S(2)}) collective-permute-start(bf16[256,1408]{1,0:T(8,128)(2,1)S(1)} %collective-permute-done.7), channel_id=1, source_target_pairs={{0,14},{2,0},{4,2},{6,4},{8,6},{10,8},{12,10},{14,12},{1,15},{3,1}... | collective-permute-start | bytes 2162696 | tf_op jit(solution)/shard_map/ppermute | solution.py:16
  340.0 29.2 %collective-permute-start.9 = (bf16[256,1408]{1,0:T(8,128)(2,1)S(1)}, bf16[256,1408]{1,0:T(8,128)(2,1)S(1)}, u32[]{:S(2)}, u32[]{:S(2)}) collective-permute-start(bf16[256,1408]{1,0:T(8,128)(2,1)S(1)} %collective-permute-done.8), channel_id=1, source_target_pairs={{0,14},{2,0},{4,2},{6,4},{8,6},{10,8},{12,10},{14,12},{1,15},{3,1}... | collective-permute-start | bytes 2162696 | tf_op jit(solution)/shard_map/ppermute | solution.py:16
  369.2 35.1 %collective-permute-start.10 = (bf16[256,1408]{1,0:T(8,128)(2,1)S(1)}, bf16[256,1408]{1,0:T(8,128)(2,1)S(1)}, u32[]{:S(2)}, u32[]{:S(2)}) collective-permute-start(bf16[256,1408]{1,0:T(8,128)(2,1)S(1)} %collective-permute-done.9), channel_id=1, source_target_pairs={{0,14},{2,0},{4,2},{6,4},{8,6},{10,8},{12,10},{14,12},{1,15},{3,1}... | collective-permute-start | bytes 2162696 | tf_op jit(solution)/shard_map/ppermute | solution.py:16
  404.3 35.4 %collective-permute-start.11 = (bf16[256,1408]{1,0:T(8,128)(2,1)S(1)}, bf16[256,1408]{1,0:T(8,128)(2,1)S(1)}, u32[]{:S(2)}, u32[]{:S(2)}) collective-permute-start(bf16[256,1408]{1,0:T(8,128)(2,1)S(1)} %collective-permute-done.10), channel_id=1, source_target_pairs={{0,14},{2,0},{4,2},{6,4},{8,6},{10,8},{12,10},{14,12},{1,15},{3,1}... | collective-permute-start | bytes 2162696 | tf_op jit(solution)/shard_map/ppermute | solution.py:16
  439.7 25.6 %collective-permute-start.12 = (bf16[256,1408]{1,0:T(8,128)(2,1)S(1)}, bf16[256,1408]{1,0:T(8,128)(2,1)S(1)}, u32[]{:S(2)}, u32[]{:S(2)}) collective-permute-start(bf16[256,1408]{1,0:T(8,128)(2,1)S(1)} %collective-permute-done.11), channel_id=1, source_target_pairs={{0,14},{2,0},{4,2},{6,4},{8,6},{10,8},{12,10},{14,12},{1,15},{3,1}... | collective-permute-start | bytes 2162696 | tf_op jit(solution)/shard_map/ppermute | solution.py:16
  465.2 27.9 %collective-permute-start.13 = (bf16[256,1408]{1,0:T(8,128)(2,1)S(1)}, bf16[256,1408]{1,0:T(8,128)(2,1)S(1)}, u32[]{:S(2)}, u32[]{:S(2)}) collective-permute-start(bf16[256,1408]{1,0:T(8,128)(2,1)S(1)} %collective-permute-done.12), channel_id=1, source_target_pairs={{0,14},{2,0},{4,2},{6,4},{8,6},{10,8},{12,10},{14,12},{1,15},{3,1}... | collective-permute-start | bytes 2162696 | tf_op jit(solution)/shard_map/ppermute | solution.py:16
  494.0 2.9 copy-start.1
  494.0 2.1 copy-start.3
  494.0 2.9 copy-start.5
  494.0 2.9 copy-start.6
  498.2 0.7 copy-start.7
  498.2 0.7 copy-start.8
  576.7 21.1 %copy-start.9 = (f32[2048]{0:T(1024)S(1)}, f32[2048]{0:T(1024)}, u32[]{:S(2)}) copy-start(f32[2048]{0:T(1024)} %param.29) | copy-start | bytes 24580
  576.7 21.1 %copy-start.10 = (f32[2048]{0:T(1024)S(1)}, f32[2048]{0:T(1024)}, u32[]{:S(2)}) copy-start(f32[2048]{0:T(1024)} %param.28) | copy-start | bytes 24580
  595.0 2.0 copy-start
Sparse Core Ops, SparseCore 0:
  9.5 149.5 all-gather.4
  161.1 120.6 all-gather.6
  292.6 18.1 all-reduce.2
  312.9 147.1 all-gather.8
  462.0 103.9 all-gather.10
  576.8 18.1 all-reduce.4
